TPU v7x, 32 devices: a whole 2x2x4 slice. The times are simulated.
32 devices in a mesh: grp: 2 (over y), sp: 4 (over z), tp: 4 (over x, core).
Axes of the slice: x: 2, y: 2, z: 4, core: 2. Of those that a mesh axis runs over, the one named last changes fastest.
Arguments:
- query_rows: bfloat16 [4096, 1024], P(('grp', 'sp'), 'tp'), parts along dimension 0, may hold values from -128 to 128
- key_rows: bfloat16 [4096, 256], P(('grp', 'sp'), 'tp'), parts along dimension 0, may hold values from -4 to 4
- value_rows: bfloat16 [4096, 256], P(('grp', 'sp'), 'tp'), parts along dimension 0, may hold values from -6 to 6
- sink_logits: float32 [16], P('tp'), may hold values from 3 to 7
- residual: bfloat16 [4096, 2048], P(('grp', 'sp', 'tp')), parts along dimension 0, may hold values from -6 to 6
- out_weight: bfloat16 [1024, 2048], P('tp'), may hold values from -0.1875 to 0.1875
- norm_gain: float32 [2048], replicated, may hold values from 0.1 to 1.9
- gate_weight: bfloat16 [16, 2048, 512], P(('sp', 'tp')), may hold values from -0.125 to 0.125
- up_weight: bfloat16 [16, 2048, 512], P(('sp', 'tp')), may hold values from -0.125 to 0.125
- down_weight: bfloat16 [16, 512, 2048], P(('sp', 'tp')), may hold values from -0.25 to 0.25
- routes: int32 [4096, 2], P(('grp', 'sp', 'tp')), parts along dimension 0, may hold values from 0 to 15, as said below
- route_weight: float32 [4096, 2], P(('grp', 'sp', 'tp')), parts along dimension 0, may hold values from 0.1 to 1
Outputs:
- layer_out: bfloat16 [4096, 2048], P(('grp', 'sp', 'tp')), parts along dimension 0
There are 2 independent parts, one for each index of `grp`. A program takes and returns all parts, laid end to end along the dimension named above; an argument that names none is the same for every part. Nothing has to cross between parts.
Inputs may be any that keep to these rules, and one draw needn't show every extreme that they name: `routes`: A token's two experts differ and lie in the same group of 4 consecutive experts. Among the 128 tokens of one device (aligned blocks of 128 rows) no expert is named more than 32 times; in every block each expert of one group, the same group for all blocks, is named exactly 32 times.
All inputs are finite; a program needn't handle non-finite values.
Results may differ from a plain program's by a relative error of at most 0.013.
Values may be sent and summed in bfloat16 or wider, within the bound.
No kernel may reach another device: no remote copies, remote signals or barrier semaphores. Data moves between devices by JAX's collectives and lax.ppermute only.
A program may use at most 64 MiB of HBM per device.

v0:
```python
import jax
import jax.numpy as jnp
from jax import lax
from jax.sharding import PartitionSpec as P

HDIM = 64
WINDOW = 128
rope_base = 10000.0
norm_eps = 1e-06


def shifted(block, axis, distance):
    devices = range(lax.axis_size(axis))
    route = [(i - distance, i) for i in devices if i - distance in devices]
    return lax.ppermute(block, axis, route)


def rotate(rows, positions, heads):
    half_dim = HDIM // 2
    values = rows.astype(jnp.float32).reshape(rows.shape[0], heads, HDIM)
    inverse = rope_base ** (-jnp.arange(half_dim, dtype=jnp.float32) / half_dim)
    angles = positions.astype(jnp.float32)[:, None] * inverse[None, :]
    cosines = jnp.cos(angles)[:, None, :]
    sines = jnp.sin(angles)[:, None, :]
    lower = values[..., :half_dim]
    upper = values[..., half_dim:]
    turned = jnp.concatenate(
        [lower * cosines - upper * sines, upper * cosines + lower * sines], axis=-1
    )
    return turned.reshape(rows.shape[0], heads * HDIM).astype(jnp.bfloat16)


def per_device(
    query_rows,
    key_rows,
    value_rows,
    sink_logits,
    residual,
    out_weight,
    norm_gain,
    gate_weight,
    up_weight,
    down_weight,
    routes,
    route_weight,
):
    tok_count = query_rows.shape[0]
    head_local = query_rows.shape[1] // HDIM
    group_local = key_rows.shape[1] // HDIM
    repeat = head_local // group_local
    first_pos = lax.axis_index("sp") * tok_count
    positions = first_pos + jnp.arange(tok_count, dtype=jnp.int32)
    rot_q = rotate(query_rows, positions, head_local)
    rot_k = rotate(key_rows, positions, group_local)
    tails = jnp.stack([rot_k[tok_count - WINDOW :], value_rows[tok_count - WINDOW :]])
    earlier = shifted(tails, "sp", 1)
    blocks = tok_count // WINDOW
    q_blocks = rot_q.reshape(blocks, WINDOW, group_local, repeat, HDIM)
    k_blocks = rot_k.reshape(blocks, WINDOW, group_local, HDIM)
    v_blocks = value_rows.reshape(blocks, WINDOW, group_local, HDIM)
    k_prev = jnp.concatenate(
        [earlier[0].reshape(1, WINDOW, group_local, HDIM), k_blocks[:-1]], axis=0
    )
    v_prev = jnp.concatenate(
        [earlier[1].reshape(1, WINDOW, group_local, HDIM), v_blocks[:-1]], axis=0
    )
    k_wide = jnp.concatenate([k_prev, k_blocks], axis=1)
    v_wide = jnp.concatenate([v_prev, v_blocks], axis=1)
    query_pos = jnp.arange(WINDOW) + WINDOW
    key_pos = jnp.arange(2 * WINDOW)
    distance = query_pos[:, None] - key_pos[None, :]
    in_band = (distance >= 0) & (distance < WINDOW)
    key_global = (
        first_pos + jnp.arange(blocks)[:, None, None] * WINDOW + key_pos[None, None, :] - WINDOW
    )
    allowed = in_band[None] & (key_global >= 0)
    scores = jnp.einsum(
        "nqgrd,nkgd->grnqk", q_blocks, k_wide, preferred_element_type=jnp.float32
    ) * HDIM ** (-0.5)
    scores = jnp.where(allowed[None, None], scores, -jnp.inf)
    sink_here = sink_logits.reshape(group_local, repeat)[:, :, None, None, None]
    largest = jnp.maximum(scores.max(axis=-1, keepdims=True), sink_here)
    exp_scores = jnp.exp(scores - largest)
    denominator = exp_scores.sum(axis=-1, keepdims=True) + jnp.exp(sink_here - largest)
    probs = (exp_scores / denominator).astype(jnp.bfloat16)
    attended = jnp.einsum("grnqk,nkgd->nqgrd", probs, v_wide, preferred_element_type=jnp.float32)
    attended = attended.astype(jnp.bfloat16).reshape(tok_count, head_local * HDIM)
    row_count = residual.shape[0]
    token_rows = lax.all_to_all(attended, "tp", split_axis=0, concat_axis=1, tiled=True)
    projected = jnp.dot(
        token_rows,
        lax.all_gather(out_weight, "tp", axis=0, tiled=True),
        preferred_element_type=jnp.float32,
    )
    stream_f = (residual.astype(jnp.float32) + projected).astype(jnp.bfloat16).astype(jnp.float32)
    normed = (
        stream_f
        * lax.rsqrt(jnp.mean(stream_f * stream_f, axis=-1, keepdims=True) + norm_eps)
        * norm_gain[None, :]
    ).astype(jnp.bfloat16)
    sp_count = lax.axis_size("sp")
    tp_count = lax.axis_size("tp")
    expert_count = sp_count * tp_count
    capacity = 4 * row_count // expert_count
    width = normed.shape[1]
    flat_expert = routes.reshape(-1)
    one_hot = (flat_expert[:, None] == jnp.arange(expert_count, dtype=jnp.int32)[None, :]).astype(
        jnp.int32
    )
    slot_rank = jnp.sum((jnp.cumsum(one_hot, axis=0) - one_hot) * one_hot, axis=1)
    slot_index = flat_expert * capacity + slot_rank
    token_of = jnp.arange(2 * row_count, dtype=jnp.int32) // 2
    outgoing = (
        jnp.zeros((expert_count * capacity, width), jnp.bfloat16)
        .at[slot_index]
        .set(normed[token_of])
    )
    outgoing = outgoing.reshape(expert_count, capacity, width)
    arrived = lax.all_to_all(outgoing, ("sp", "tp"), split_axis=0, concat_axis=0, tiled=True)
    flat_rows = arrived.reshape(-1, width)
    gate_out = jnp.dot(flat_rows, gate_weight[0], preferred_element_type=jnp.float32)
    up_out = jnp.dot(flat_rows, up_weight[0], preferred_element_type=jnp.float32)
    hidden = (jax.nn.silu(gate_out) * up_out).astype(jnp.bfloat16)
    produced = jnp.dot(hidden, down_weight[0], preferred_element_type=jnp.float32).astype(
        jnp.bfloat16
    )
    returned = lax.all_to_all(
        produced.reshape(arrived.shape), ("sp", "tp"), split_axis=0, concat_axis=0, tiled=True
    )
    gathered = returned.reshape(expert_count * capacity, width)[slot_index].astype(jnp.float32)
    weighted = gathered * route_weight.reshape(-1)[:, None]
    combined = weighted.reshape(row_count, 2, width).sum(axis=1)
    return (stream_f + combined).astype(jnp.bfloat16)


def solution(mesh):
    in_specs = (
        P(("grp", "sp"), "tp"),
        P(("grp", "sp"), "tp"),
        P(("grp", "sp"), "tp"),
        P("tp"),
        P(("grp", "sp", "tp"), None),
        P("tp", None),
        P(),
        P(("sp", "tp"), None, None),
        P(("sp", "tp"), None, None),
        P(("sp", "tp"), None, None),
        P(("grp", "sp", "tp"), None),
        P(("grp", "sp", "tp"), None),
    )
    out_specs = P(("grp", "sp", "tp"), None)
    return jax.shard_map(
        per_device, mesh=mesh, in_specs=in_specs, out_specs=out_specs, check_vma=False
    )
```

profile of v0, /device:TPU:11, one launch (start us, length us, event | category | flops | bytes accessed | tf_op | source)
XLA Modules:
  0.0 195.3 jit_solution(5464959872850920019)
XLA Ops:
  6.5 0.7 all-gather.2.cloned.1.call-update
  7.3 0.9 bitcast_convert_fusion
  8.2 0.3 fusion.38
  8.5 0.7 slice_bitcast_fusion.4
  9.3 3.2 %collective-permute-start = (bf16[2,128,64]{1,2,0:T(8,128)(2,1)S(1)}, bf16[2,128,64]{1,2,0:T(8,128)(2,1)S(1)}, u32[]{:S(2)}, u32[]{:S(2)}) collective-permute-start(bf16[2,128,64]{1,2,0:T(8,128)(2,1)S(1)} %pad_maximum_fusion), channel_id=1, source_target_pairs={{0,4},{4,8},{8,12},{1,5},{5,9},{9,13},{2,6},{6,10},{10,14},{3,7},{... | collective-permute-start | bytes 98312 | tf_op jit(solution)/shard_map/ppermute | solution.py:15
  12.5 0.8 copy.25
  13.4 0.1 eq.25
  13.5 0.1 copy.21
  13.8 0.6 reduce-window.6
  14.3 0.2 slice_reduce_fusion
  14.8 0.3 multiply_cosine_fusion
  15.2 0.2 broadcast_and_fusion
  15.7 0.1 mul.180
  15.9 0.5 fusion.47
  16.5 0.3 fusion.7
  16.9 1.2 convolution_convert_fusion.1
  18.1 4.5 %all-to-all-start = ((bf16[4,128,256]{1,2,0:T(8,128)(2,1)}), bf16[4,128,256]{1,2,0:T(8,128)(2,1)S(1)}, u32[]{:S(2)}, u32[]{:S(2)}) async-start(bf16[4,128,256]{1,2,0:T(8,128)(2,1)} %bitcast.20), calls=%async_computation | async-start | bytes 524288 | tf_op jit(solution)/shard_map/all_to_all | solution.py:89
  22.5 7.4 %all-to-all-done = bf16[4,128,256]{1,2,0:T(8,128)(2,1)S(1)} async-done(((bf16[4,128,256]{1,2,0:T(8,128)(2,1)}), bf16[4,128,256]{1,2,0:T(8,128)(2,1)S(1)}, u32[]{:S(2)}, u32[]{:S(2)}) %all-to-all-start) | async-done | bytes 262176 | tf_op jit(solution)/shard_map/all_to_all | solution.py:89
  29.9 16.9 %all-gather.2.cloned.1.call-done = bf16[1024,2048]{1,0:T(8,128)(2,1)} async-done(((bf16[256,2048]{1,0:T(8,128)(2,1)}), bf16[1024,2048]{1,0:T(8,128)(2,1)}) %all-gather.2.cloned.1.call-update) | async-done | bytes 4194320 | tf_op jit(solution)/shard_map/all_gather | solution.py:92
  46.9 3.1 %multiply_reduce_fusion.1 = (f32[128]{0:T(128)S(1)}, f32[128,2048]{1,0:T(8,128)S(1)}) fusion(bf16[128,1024]{0,1:T(8,128)(2,1)S(1)} %bitcast.116, bf16[1024,2048]{1,0:T(8,128)(2,1)} %all-gather.2.cloned.1.call-done, bf16[128,2048]{1,0:T(8,128)(2,1)} %param.16), kind=kOutput, calls=%fused_computation.25 | convolution fusion | flops 538443648 | bytes 6029824 | tf_op jit(solution)/shard_map/dot_general | solution.py:90
  50.0 1.0 multiply_convert_fusion
  51.0 7.3 %scatter_custom_fusion = bf16[512,2048]{1,0:T(8,128)(2,1)} fusion(s32[256]{0:T(256)S(1)} %bitcast.119, bf16[128,2048]{1,0:T(8,128)(2,1)} %multiply_convert_fusion, s32[1024]{0:T(1024)S(1)} %pad_clamp_fusion.1, bf16[]{:T(256)} %constant.56.clone.1), kind=kCustom, calls=%fused_computation.21 | custom fusion | bytes 2097664 | tf_op jit(solution)/shard_map/scatter | solution.py:116
  58.3 53.3 %all_to_all.29 = bf16[16,32,2048]{2,1,0:T(8,128)(2,1)S(1)} all-to-all(bf16[16,32,2048]{2,1,0:T(8,128)(2,1)} %bitcast.112), channel_id=1, replica_groups=mesh['grp'=2,'sp'=4,'tp'=4] {'sp','tp'}, dimensions={0} | all-to-all | bytes 4194304 | tf_op jit(solution)/shard_map/all_to_all | solution.py:119
  111.7 1.3 copy-done.1
  112.9 2.2 %fusion.5 = f32[512,512]{1,0:T(8,128)} fusion(bf16[512,2048]{1,0:T(8,128)(2,1)S(1)} %bitcast.114, bf16[1,2048,512]{2,1,0:T(8,128)(2,1)S(1)} %copy-done.8), kind=kOutput, calls=%fused_computation.11 | convolution fusion | flops 1073741824 | bytes 5242880 | tf_op jit(solution)/shard_map/dot_general | solution.py:121
  115.2 6.3 %convolution_convert_fusion = bf16[512,2048]{1,0:T(8,128)(2,1)} fusion(bf16[1,512,2048]{2,1,0:T(8,128)(2,1)S(1)} %copy-done, bf16[512,2048]{1,0:T(8,128)(2,1)} %bitcast.115, bf16[1,2048,512]{2,1,0:T(8,128)(2,1)} %param.20, f32[512,512]{1,0:T(8,128)} %fusion.5), kind=kOutput, calls=%fused_computation.3 | convolution fusion | flops 2150105088 | bytes 9437184 | tf_op jit(solution)/shard_map/dot_general | solution.py:124
  121.5 5.1 %all-to-all-start.2 = ((bf16[16,32,2048]{2,1,0:T(8,128)(2,1)}), bf16[16,32,2048]{2,1,0:T(8,128)(2,1)}, u32[]{:S(2)}, u32[]{:S(2)}) async-start(bf16[16,32,2048]{2,1,0:T(8,128)(2,1)} %bitcast.113), calls=%async_computation.2 | async-start | bytes 4194304 | tf_op jit(solution)/shard_map/all_to_all | solution.py:127
  126.7 47.4 %all-to-all-done.2 = bf16[16,32,2048]{2,1,0:T(8,128)(2,1)} async-done(((bf16[16,32,2048]{2,1,0:T(8,128)(2,1)}), bf16[16,32,2048]{2,1,0:T(8,128)(2,1)}, u32[]{:S(2)}, u32[]{:S(2)}) %all-to-all-start.2) | async-done | bytes 2097184 | tf_op jit(solution)/shard_map/all_to_all | solution.py:127
  174.1 5.2 %gather_fusion = bf16[256,2048]{1,0:T(8,128)(2,1)} fusion(bf16[512,2048]{1,0:T(8,128)(2,1)} %bitcast.33, s32[1024]{0:T(1024)S(1)} %pad_clamp_fusion), kind=kCustom, calls=%fused_computation.1 | custom fusion | bytes 2098176 | tf_op jit(solution)/shard_map/gather | solution.py:130
  179.3 3.4 %reshape.391 = f32[128,2,2048]{2,1,0:T(2,128)} reshape(bf16[256,2048]{1,0:T(8,128)(2,1)} %gather_fusion) | data formatting | bytes 3145728 | tf_op jit(solution)/shard_map/convert_element_type | solution.py:130
  182.7 4.8 %multiply_reduce_fusion = f32[128,2048]{1,0:T(8,128)S(1)} fusion(f32[128,2,2048]{2,1,0:T(2,128)} %reshape.391, f32[128,2]{1,0:T(8,128)S(1)} %copy.28), kind=kLoop, calls=%fused_computation.13 | loop fusion | flops 786432 | bytes 3146752 | tf_op jit(solution)/shard_map/reduce_sum | solution.py:132
  187.5 0.9 add_convert_fusion
  (54 shorter events, 1.1 us)
Async XLA Ops:
  6.5 108.6 %copy-start = (bf16[1,512,2048]{2,1,0:T(8,128)(2,1)S(1)}, bf16[1,512,2048]{2,1,0:T(8,128)(2,1)}, u32[]{:S(2)}) copy-start(bf16[1,512,2048]{2,1,0:T(8,128)(2,1)} %param.21) | copy-start | bytes 6291460
  6.5 8.2 %copy-start.5 = (s32[128,2]{0,1:T(2,128)S(1)}, s32[128,2]{0,1:T(2,128)}, u32[]{:S(2)}) copy-start(s32[128,2]{0,1:T(2,128)} %param.22) | copy-start | bytes 3076
  6.5 7.0 %copy-start.2 = (bf16[512,256]{1,0:T(8,128)(2,1)S(1)}, bf16[512,256]{1,0:T(8,128)(2,1)}, u32[]{:S(2)}) copy-start(bf16[512,256]{1,0:T(8,128)(2,1)} %param.12) | copy-start | bytes 786436
  6.5 40.3 %all-gather.2.cloned.1.call-start = ((), (), s32[]{:S(2)}) async-start(), calls=%async_computation.3 | async-start | bytes 5242880 | tf_op jit(solution)/shard_map/all_gather | solution.py:92
  7.3 8.2 %copy-start.3 = (bf16[512,64]{0,1:T(8,128)(2,1)S(1)}, bf16[512,64]{0,1:T(8,128)(2,1)}, u32[]{:S(2)}) copy-start(bf16[512,64]{0,1:T(8,128)(2,1)} %param.14) | copy-start | bytes 196612
  7.3 8.2 %slice-start = ((bf16[512,64]{0,1:T(8,128)(2,1)}), bf16[384,64]{0,1:T(8,128)(2,1)S(1)}, s32[]{:S(2)}) async-start(bf16[512,64]{0,1:T(8,128)(2,1)} %param.14), calls=%async_computation.4 | async-start | bytes 98304 | tf_op jit(solution)/shard_map/slice | solution.py:65
  9.3 6.6 %collective-permute-start = (bf16[2,128,64]{1,2,0:T(8,128)(2,1)S(1)}, bf16[2,128,64]{1,2,0:T(8,128)(2,1)S(1)}, u32[]{:S(2)}, u32[]{:S(2)}) collective-permute-start(bf16[2,128,64]{1,2,0:T(8,128)(2,1)S(1)} %pad_maximum_fusion), channel_id=1, source_target_pairs={{0,4},{4,8},{8,12},{1,5},{5,9},{9,13},{2,6},{6,10},{10,14},{3,7},{... | collective-permute-start | bytes 98312 | tf_op jit(solution)/shard_map/ppermute | solution.py:15
  15.5 0.9 copy-start.6
  18.1 11.8 %all-to-all-start = ((bf16[4,128,256]{1,2,0:T(8,128)(2,1)}), bf16[4,128,256]{1,2,0:T(8,128)(2,1)S(1)}, u32[]{:S(2)}, u32[]{:S(2)}) async-start(bf16[4,128,256]{1,2,0:T(8,128)(2,1)} %bitcast.20), calls=%async_computation | async-start | bytes 524288 | tf_op jit(solution)/shard_map/all_to_all | solution.py:89
  46.9 3.2 %copy-start.4 = (f32[2048]{0:T(1024)S(1)}, f32[2048]{0:T(1024)}, u32[]{:S(2)}) copy-start(f32[2048]{0:T(1024)} %param.18) | copy-start | bytes 24580
  58.3 54.6 %copy-start.8 = (bf16[1,2048,512]{2,1,0:T(8,128)(2,1)S(1)}, bf16[1,2048,512]{2,1,0:T(8,128)(2,1)}, u32[]{:S(2)}) copy-start(bf16[1,2048,512]{2,1,0:T(8,128)(2,1)} %param.19) | copy-start | bytes 6291460
  111.6 1.3 copy-start.1
  121.5 5.1 %copy-start.7 = (f32[128,2]{0,1:T(2,128)S(1)}, f32[128,2]{0,1:T(2,128)}, u32[]{:S(2)}) copy-start(f32[128,2]{0,1:T(2,128)} %param.23) | copy-start | bytes 3076
  121.5 52.7 %all-to-all-start.2 = ((bf16[16,32,2048]{2,1,0:T(8,128)(2,1)}), bf16[16,32,2048]{2,1,0:T(8,128)(2,1)}, u32[]{:S(2)}, u32[]{:S(2)}) async-start(bf16[16,32,2048]{2,1,0:T(8,128)(2,1)} %bitcast.113), calls=%async_computation.2 | async-start | bytes 4194304 | tf_op jit(solution)/shard_map/all_to_all | solution.py:127
Sparse Core Ops, SparseCore 0:
  8.9 37.9 all-gather.1
where the time goes:
time: 196 us; the launch traced here: 195 us
  waiting for transfers between devices  72.4 us (37%)
  blocking collectives  53.3 us (27%)
  local copies, waits for them, and re-layouts  19.8 us (10%)
  between operations  13.7 us (7%)
  matrix products  13.4 us (7%)
  starting transfers between devices  12.8 us (7%)
  other arithmetic  9.91 us (5%)
    all_to_all x1, blocking collectives, per_device(): lax.all_to_all(outgoing, ('sp', 'tp'), split_axis=0, concat_axis=0, tiled...  53.3 us
    all_to_all x1, waiting for transfers between devices, per_device(): lax.all_to_all(produced.reshape(arrived.shape), ('sp', 'tp'), split_axis=...  47.4 us
    all_gather x1, waiting for transfers between devices, per_device(): lax.all_gather(out_weight, 'tp', axis=0, tiled=True)  16.9 us
    all_to_all x1, waiting for transfers between devices, per_device(): lax.all_to_all(attended, 'tp', split_axis=0, concat_axis=1, tiled=True)  7.37 us
    scatter x1, local copies, waits for them, and re-layouts, per_device(): outgoing = jnp.zeros((expert_count * capacity, width), jnp.bfloat16).at[s...  7.33 us
    dot_general x1, matrix products, per_device(): jnp.dot(hidden, down_weight[0], preferred_element_type=jnp.float32)  6.28 us
    gather x1, local copies, waits for them, and re-layouts, per_device(): returned.reshape(expert_count * capacity, width)[slot_index]  5.2 us
    all_to_all x1, starting transfers between devices, per_device(): lax.all_to_all(produced.reshape(arrived.shape), ('sp', 'tp'), split_axis=...  5.14 us
  transfers between devices with their start and end apart: 4, of which 3 were waited for; matrix products, arithmetic and copies ran while one was open for 4% of the time, Pallas kernels for 0%

commit v1 on v0

--- a/solution.py
+++ b/solution.py
@@ -89,7 +89,9 @@
     token_rows = lax.all_to_all(attended, "tp", split_axis=0, concat_axis=1, tiled=True)
     projected = jnp.dot(
         token_rows,
-        lax.all_gather(out_weight, "tp", axis=0, tiled=True),
+        jnp.concatenate(
+            lax.all_to_all(jnp.stack([out_weight] * lax.axis_size("tp")), "tp", 0, 0), axis=0
+        ),
         preferred_element_type=jnp.float32,
     )
     stream_f = (residual.astype(jnp.float32) + projected).astype(jnp.bfloat16).astype(jnp.float32)

time: 196 us -> 217 us (1.11)
  waiting for transfers between devices: 72.4 us -> 92.2 us
  between operations: 13.7 us -> 0.29 us
  blocking collectives: 53.3 us -> 62.9 us
  local copies, waits for them, and re-layouts: 19.8 us -> 23.5 us
  starting transfers between devices: 12.8 us -> 15.2 us
    all_to_all x1, waiting for transfers between devices: 7.37 us -> 44.8 us  [per_device(): lax.all_to_all(jnp.stack([out_weight] * lax.axis_size('tp')), 'tp', 0, 0)]
    all_gather x1 -> x0, waiting for transfers between devices: 16.9 us -> none  [per_device(): lax.all_gather(out_weight, 'tp', axis=0, tiled=True)]
    all_to_all x0 -> x1, blocking collectives: none -> 8.84 us  [per_device(): lax.all_to_all(attended, 'tp', split_axis=0, concat_axis=1, tiled=True)]
    another operation x1 -> x2, local copies, waits for them, and re-layouts: 0.01 us -> 2.5 us  [the longest x1 2.49 us: per_device(): jnp.stack([out_weight] * lax.axis_size('tp'))]
    all_to_all x1, starting transfers between devices: 4.47 us -> 6.81 us  [per_device(): lax.all_to_all(jnp.stack([out_weight] * lax.axis_size('tp')), 'tp', 0, 0)]
  transfers between devices with their start and end apart: 4 -> 3, of which waited for: 3 -> 2; matrix products, arithmetic and copies ran while one was open for 4% -> 2% of each run, Pallas kernels for 0% -> 0%
where the time goes in v1:
time: 217 us
  waiting for transfers between devices  92.2 us (42%)
  blocking collectives  62.9 us (29%)
  local copies, waits for them, and re-layouts  23.5 us (11%)
  starting transfers between devices  15.2 us (7%)
  matrix products  12.6 us (6%)
  other arithmetic  10.1 us (5%)
    all_to_all x1, blocking collectives, per_device(): lax.all_to_all(outgoing, ('sp', 'tp'), split_axis=0, concat_axis=0, tiled...  54 us
    all_to_all x1, waiting for transfers between devices, per_device(): lax.all_to_all(produced.reshape(arrived.shape), ('sp', 'tp'), split_axis=...  47.4 us
    all_to_all x1, waiting for transfers between devices, per_device(): lax.all_to_all(jnp.stack([out_weight] * lax.axis_size('tp')), 'tp', 0, 0)  44.8 us
    all_to_all x1, blocking collectives, per_device(): lax.all_to_all(attended, 'tp', split_axis=0, concat_axis=1, tiled=True)  8.84 us
    scatter x1, local copies, waits for them, and re-layouts, per_device(): outgoing = jnp.zeros((expert_count * capacity, width), jnp.bfloat16).at[s...  7.36 us
    all_to_all x1, starting transfers between devices, per_device(): lax.all_to_all(jnp.stack([out_weight] * lax.axis_size('tp')), 'tp', 0, 0)  6.81 us
    dot_general x1, matrix products, per_device(): jnp.dot(hidden, down_weight[0], preferred_element_type=jnp.float32)  6.27 us
    gather x1, local copies, waits for them, and re-layouts, per_device(): returned.reshape(expert_count * capacity, width)[slot_index]  5.2 us
  transfers between devices with their start and end apart: 3, of which 2 were waited for; matrix products, arithmetic and copies ran while one was open for 2% of the time, Pallas kernels for 0%

profile of v1, /device:TPU:11, one launch (start us, length us, event | category | flops | bytes accessed | tf_op | source)
XLA Modules:
  0.0 216.7 jit_solution(2857090912306702190)
XLA Ops:
  0.0 1.0 bitcast_convert_fusion
  1.1 0.7 slice_bitcast_fusion.4
  1.8 0.3 fusion.40
  2.1 3.2 %collective-permute-start = (bf16[2,128,64]{1,2,0:T(8,128)(2,1)S(1)}, bf16[2,128,64]{1,2,0:T(8,128)(2,1)S(1)}, u32[]{:S(2)}, u32[]{:S(2)}) collective-permute-start(bf16[2,128,64]{1,2,0:T(8,128)(2,1)S(1)} %pad_maximum_fusion), channel_id=1, source_target_pairs={{0,4},{4,8},{8,12},{1,5},{5,9},{9,13},{2,6},{6,10},{10,14},{3,7},{... | collective-permute-start | bytes 98312 | tf_op jit(solution)/shard_map/ppermute | solution.py:15
  5.4 0.3 multiply_cosine_fusion
  5.8 1.1 copy.22
  7.0 0.2 broadcast_and_fusion
  7.4 0.5 fusion.49
  8.0 0.3 fusion.8
  8.4 0.5 convolution_convert_fusion.1
  8.9 0.9 copy.25
  9.8 8.8 %all_to_all.31 = bf16[4,128,256]{2,1,0:T(8,128)(2,1)S(1)} all-to-all(bf16[4,128,256]{2,1,0:T(8,128)(2,1)} %copy.25), channel_id=1, replica_groups=mesh['grp'=2,'sp'=4,'tp'=4] {'tp'}, dimensions={0} | all-to-all | bytes 524288 | tf_op jit(solution)/shard_map/all_to_all | solution.py:89
  18.6 2.5 %stack.19 = bf16[4,256,2048]{2,1,0:T(8,128)(2,1)} broadcast(bf16[256,2048]{1,0:T(8,128)(2,1)S(1)} %copy-done.2), dimensions={1,2} | broadcast | bytes 5242880 | tf_op jit(solution)/shard_map/stack | solution.py:93
  21.1 6.8 %all-to-all-start.1 = ((bf16[4,256,2048]{2,1,0:T(8,128)(2,1)}), bf16[4,256,2048]{2,1,0:T(8,128)(2,1)}, u32[]{:S(2)}, u32[]{:S(2)}) async-start(bf16[4,256,2048]{2,1,0:T(8,128)(2,1)} %stack.19), calls=%async_computation.1 | async-start | bytes 8388608 | tf_op jit(solution)/shard_map/all_to_all | solution.py:93
  28.2 0.1 eq.29
  28.5 0.1 mul.180
  28.6 0.6 reduce-window.6
  29.2 0.2 slice_reduce_fusion
  29.6 44.8 %all-to-all-done.1 = bf16[4,256,2048]{2,1,0:T(8,128)(2,1)} async-done(((bf16[4,256,2048]{2,1,0:T(8,128)(2,1)}), bf16[4,256,2048]{2,1,0:T(8,128)(2,1)}, u32[]{:S(2)}, u32[]{:S(2)}) %all-to-all-start.1) | async-done | bytes 4194336 | tf_op jit(solution)/shard_map/all_to_all | solution.py:93
  74.3 3.1 %multiply_reduce_fusion.1 = (f32[128]{0:T(128)S(1)}, f32[128,2048]{1,0:T(8,128)S(1)}) fusion(bf16[4,256,2048]{2,1,0:T(8,128)(2,1)} %all-to-all-done.1, bf16[4,128,256]{2,1,0:T(8,128)(2,1)S(1)} %all_to_all.31, bf16[128,2048]{1,0:T(8,128)(2,1)} %param.16), kind=kOutput, calls=%fused_computation.26 | convolution fusion | flops 538443648 | bytes 6029824 | tf_op jit(solution)/shard_map/dot_general | solution.py:90
  77.5 0.9 multiply_convert_fusion
  78.5 7.4 %scatter_custom_fusion = bf16[512,2048]{1,0:T(8,128)(2,1)} fusion(s32[256]{0:T(256)S(1)} %bitcast.127, bf16[128,2048]{1,0:T(8,128)(2,1)} %multiply_convert_fusion, s32[1024]{0:T(1024)S(1)} %pad_clamp_fusion.1, bf16[]{:T(256)} %constant.56.clone.1), kind=kCustom, calls=%fused_computation.22 | custom fusion | bytes 2097664 | tf_op jit(solution)/shard_map/scatter | solution.py:118
  85.8 54.0 %all_to_all.32 = bf16[16,32,2048]{2,1,0:T(8,128)(2,1)S(1)} all-to-all(bf16[16,32,2048]{2,1,0:T(8,128)(2,1)} %bitcast.121), channel_id=1, replica_groups=mesh['grp'=2,'sp'=4,'tp'=4] {'sp','tp'}, dimensions={0} | all-to-all | bytes 4194304 | tf_op jit(solution)/shard_map/all_to_all | solution.py:121
  139.8 1.3 copy-done.1
  141.1 2.2 %fusion.6 = f32[512,512]{1,0:T(8,128)} fusion(bf16[512,2048]{1,0:T(8,128)(2,1)S(1)} %bitcast.123, bf16[1,2048,512]{2,1,0:T(8,128)(2,1)S(1)} %copy-done.8), kind=kOutput, calls=%fused_computation.12 | convolution fusion | flops 1073741824 | bytes 5242880 | tf_op jit(solution)/shard_map/dot_general | solution.py:123
  143.4 6.3 %convolution_convert_fusion = bf16[512,2048]{1,0:T(8,128)(2,1)} fusion(bf16[1,512,2048]{2,1,0:T(8,128)(2,1)S(1)} %copy-done, bf16[512,2048]{1,0:T(8,128)(2,1)} %bitcast.124, bf16[1,2048,512]{2,1,0:T(8,128)(2,1)} %param.20, f32[512,512]{1,0:T(8,128)} %fusion.6), kind=kOutput, calls=%fused_computation.3 | convolution fusion | flops 2150105088 | bytes 9437184 | tf_op jit(solution)/shard_map/dot_general | solution.py:126
  149.6 5.2 %all-to-all-start.3 = ((bf16[16,32,2048]{2,1,0:T(8,128)(2,1)}), bf16[16,32,2048]{2,1,0:T(8,128)(2,1)}, u32[]{:S(2)}, u32[]{:S(2)}) async-start(bf16[16,32,2048]{2,1,0:T(8,128)(2,1)} %bitcast.122), calls=%async_computation.3 | async-start | bytes 4194304 | tf_op jit(solution)/shard_map/all_to_all | solution.py:129
  154.9 47.4 %all-to-all-done.3 = bf16[16,32,2048]{2,1,0:T(8,128)(2,1)} async-done(((bf16[16,32,2048]{2,1,0:T(8,128)(2,1)}), bf16[16,32,2048]{2,1,0:T(8,128)(2,1)}, u32[]{:S(2)}, u32[]{:S(2)}) %all-to-all-start.3) | async-done | bytes 2097184 | tf_op jit(solution)/shard_map/all_to_all | solution.py:129
  202.3 5.2 %gather_fusion = bf16[256,2048]{1,0:T(8,128)(2,1)} fusion(bf16[512,2048]{1,0:T(8,128)(2,1)} %bitcast.33, s32[1024]{0:T(1024)S(1)} %pad_clamp_fusion), kind=kCustom, calls=%fused_computation.1 | custom fusion | bytes 2098176 | tf_op jit(solution)/shard_map/gather | solution.py:132
  207.5 3.4 %reshape.394 = f32[128,2,2048]{2,1,0:T(2,128)} reshape(bf16[256,2048]{1,0:T(8,128)(2,1)} %gather_fusion) | data formatting | bytes 3145728 | tf_op jit(solution)/shard_map/convert_element_type | solution.py:132
  210.9 4.8 %multiply_reduce_fusion = f32[128,2048]{1,0:T(8,128)S(1)} fusion(f32[128,2,2048]{2,1,0:T(2,128)} %reshape.394, f32[128,2]{1,0:T(8,128)S(1)} %copy.30), kind=kLoop, calls=%fused_computation.14 | loop fusion | flops 786432 | bytes 3146752 | tf_op jit(solution)/shard_map/reduce_sum | solution.py:134
  215.7 0.9 add_convert_fusion
  (54 shorter events, 1.2 us)
Async XLA Ops:
  0.0 143.4 %copy-start = (bf16[1,512,2048]{2,1,0:T(8,128)(2,1)S(1)}, bf16[1,512,2048]{2,1,0:T(8,128)(2,1)}, u32[]{:S(2)}) copy-start(bf16[1,512,2048]{2,1,0:T(8,128)(2,1)} %param.21) | copy-start | bytes 6291460
  0.0 7.3 %copy-start.3 = (bf16[512,64]{0,1:T(8,128)(2,1)S(1)}, bf16[512,64]{0,1:T(8,128)(2,1)}, u32[]{:S(2)}) copy-start(bf16[512,64]{0,1:T(8,128)(2,1)} %param.14) | copy-start | bytes 196612
  0.0 7.4 %slice-start = ((bf16[512,64]{0,1:T(8,128)(2,1)}), bf16[384,64]{0,1:T(8,128)(2,1)S(1)}, s32[]{:S(2)}) async-start(bf16[512,64]{0,1:T(8,128)(2,1)} %param.14), calls=%async_computation.4 | async-start | bytes 98304 | tf_op jit(solution)/shard_map/slice | solution.py:65
  2.1 5.3 %collective-permute-start = (bf16[2,128,64]{1,2,0:T(8,128)(2,1)S(1)}, bf16[2,128,64]{1,2,0:T(8,128)(2,1)S(1)}, u32[]{:S(2)}, u32[]{:S(2)}) collective-permute-start(bf16[2,128,64]{1,2,0:T(8,128)(2,1)S(1)} %pad_maximum_fusion), channel_id=1, source_target_pairs={{0,4},{4,8},{8,12},{1,5},{5,9},{9,13},{2,6},{6,10},{10,14},{3,7},{... | collective-permute-start | bytes 98312 | tf_op jit(solution)/shard_map/ppermute | solution.py:15
  7.3 0.7 copy-start.6
  8.4 10.2 %copy-start.2 = (bf16[256,2048]{1,0:T(8,128)(2,1)S(1)}, bf16[256,2048]{1,0:T(8,128)(2,1)}, u32[]{:S(2)}) copy-start(bf16[256,2048]{1,0:T(8,128)(2,1)} %param.17) | copy-start | bytes 3145732
  21.1 6.8 %copy-start.5 = (s32[128,2]{0,1:T(2,128)S(1)}, s32[128,2]{0,1:T(2,128)}, u32[]{:S(2)}) copy-start(s32[128,2]{0,1:T(2,128)} %param.22) | copy-start | bytes 3076
  21.1 53.2 %all-to-all-start.1 = ((bf16[4,256,2048]{2,1,0:T(8,128)(2,1)}), bf16[4,256,2048]{2,1,0:T(8,128)(2,1)}, u32[]{:S(2)}, u32[]{:S(2)}) async-start(bf16[4,256,2048]{2,1,0:T(8,128)(2,1)} %stack.19), calls=%async_computation.1 | async-start | bytes 8388608 | tf_op jit(solution)/shard_map/all_to_all | solution.py:93
  29.6 47.9 %copy-start.4 = (f32[2048]{0:T(1024)S(1)}, f32[2048]{0:T(1024)}, u32[]{:S(2)}) copy-start(f32[2048]{0:T(1024)} %param.18) | copy-start | bytes 24580
  85.8 55.3 %copy-start.8 = (bf16[1,2048,512]{2,1,0:T(8,128)(2,1)S(1)}, bf16[1,2048,512]{2,1,0:T(8,128)(2,1)}, u32[]{:S(2)}) copy-start(bf16[1,2048,512]{2,1,0:T(8,128)(2,1)} %param.19) | copy-start | bytes 6291460
  139.8 1.3 copy-start.1
  149.6 5.2 %copy-start.7 = (f32[128,2]{0,1:T(2,128)S(1)}, f32[128,2]{0,1:T(2,128)}, u32[]{:S(2)}) copy-start(f32[128,2]{0,1:T(2,128)} %param.23) | copy-start | bytes 3076
  149.6 52.7 %all-to-all-start.3 = ((bf16[16,32,2048]{2,1,0:T(8,128)(2,1)}), bf16[16,32,2048]{2,1,0:T(8,128)(2,1)}, u32[]{:S(2)}, u32[]{:S(2)}) async-start(bf16[16,32,2048]{2,1,0:T(8,128)(2,1)} %bitcast.122), calls=%async_computation.3 | async-start | bytes 4194304 | tf_op jit(solution)/shard_map/all_to_all | solution.py:129
